TPU v7x, 32 devices: a whole 2x2x4 slice. The times are simulated.
32 devices in a mesh: sp: 16 (over z, y, x), tp: 2 (over core).
Axes of the slice: x: 2, y: 2, z: 4, core: 2. Of those that a mesh axis runs over, the one named last changes fastest.
Arguments:
- tokens: bfloat16 [6144, 2048], P('sp', 'tp'), may hold values from -40 to 40
- mix_gain: float32 [2048], replicated, may hold values from 0.1 to 1.9
- w_pool_in: bfloat16 [2048, 1024], P(None, 'tp'), may hold values from -0.125 to 0.125
- w_qlat: bfloat16 [2048, 512], P(None, 'tp'), may hold values from -0.125 to 0.125
- w_kvlat: bfloat16 [2048, 512], P(None, 'tp'), may hold values from -0.125 to 0.125
- w_krope: bfloat16 [2048, 64], replicated, may hold values from -0.125 to 0.125
- q_gain: float32 [512], replicated, may hold values from 1 to 60
- kv_gain: float32 [512], replicated, may hold values from 0.1 to 1.9
- w_q_content: bfloat16 [512, 2048], P(None, 'tp'), may hold values from -0.25 to 0.25
- w_q_rotary: bfloat16 [512, 1024], P(None, 'tp'), may hold values from -0.25 to 0.25
- w_key: bfloat16 [512, 2048], P(None, 'tp'), may hold values from -0.25 to 0.25
- w_value: bfloat16 [512, 2048], P(None, 'tp'), may hold values from -0.25 to 0.25
- pool_mix: bfloat16 [8, 128, 128], replicated, may hold values from -0.5 to 0.5
- pool_scale: float32 [1024], replicated, may hold values from 0.1 to 1.9
- w_out_pool: bfloat16 [1024, 2048], P('tp'), may hold values from -0.109375 to 0.109375
- w_out_attn: bfloat16 [2048, 2048], P('tp'), may hold values from -0.25 to 0.25
Outputs:
- layer_out: bfloat16 [6144, 2048], P(('sp', 'tp'))
- log_total: float32 [6144, 16], P('sp', 'tp')
All inputs are finite; a program needn't handle non-finite values.
Results may differ from a plain program's by a relative error of at most 0.015.
The roundings to bfloat16 on the way count: a program that leaves them out, or rounds other values in their place, can miss the bound.
Values may be sent and summed in bfloat16 or wider, within the bound.
A program may use at most 64 MiB of HBM per device.

v0:
```python
import functools
import math

import jax
import jax.numpy as jnp
from jax import lax
from jax.experimental import pallas as pl
from jax.experimental.pallas import tpu as pltpu
from jax.sharding import PartitionSpec as P

NOPE = 128
ROPE = 64
VDIM = 128
GROUP_DIM = 128
WIDEST = 16
SPAN = 16
MESH = pl.DeviceIdType.MESH


eps_norm = 1e-06
rope_base = 10000.0
masked_score = -1e30


def shifted(value, axis, steps):
    count = lax.axis_size(axis)
    leading, last = (max(0, -steps), min(count, count - steps))
    return lax.ppermute(value, axis, [(source, source + steps) for source in range(leading, last)])


def tables(positions, rotary_width):
    half_width = rotary_width // 2
    frequency = rope_base ** (-jnp.arange(half_width, dtype=jnp.float32) * 2.0 / rotary_width)
    angles = positions.astype(jnp.float32)[:, None] * frequency[None, :]
    return (jnp.cos(angles), jnp.sin(angles))


def rotate(vectors, cosine, sine_table):
    half_width = vectors.shape[-1] // 2
    first_half = vectors[..., :half_width]
    second_half = vectors[..., half_width:]
    return jnp.concatenate(
        [
            first_half * cosine - second_half * sine_table,
            second_half * cosine + first_half * sine_table,
        ],
        axis=-1,
    )


def latent_norm(latent, gain_vector):
    latent_values = latent.astype(jnp.float32)
    inverse = lax.rsqrt(jnp.mean(latent_values * latent_values, axis=-1, keepdims=True) + eps_norm)
    return (latent_values * inverse * gain_vector).astype(jnp.bfloat16)


QUAD = 4


def attend_kernel(
    seq_count, tp_size, query_ref, packed_ref, w_key_ref, w_value_ref, out_ref, log_ref,
    blocks, queries, peak_scr, total_scr, sum_scr, give, take, log_give, log_take,
    ici_recv, core_recv, z_send, near_send, far_send, core_send, swap_send, swap_recv,
):
    heads, rows, depth = query_ref.shape
    half_heads = heads // 2
    own_width = half_heads * NOPE
    latent_width = w_key_ref.shape[0]
    layers = SPAN // QUAD
    scale = (NOPE + ROPE) ** (-0.5)
    factor = scale * math.log2(math.e)
    part = rows // tp_size

    place = lax.axis_index("sp")
    core = lax.axis_index("tp")
    sequence = place % seq_count
    rank = place // seq_count
    z, y, x = rank // QUAD, (rank % QUAD) // 2, rank % 2
    low = jnp.minimum(rank, SPAN - 1 - rank)
    high = SPAN - 1 - low
    side = rank // (SPAN // 2)
    near_x, near_y = 1 - core % 2, core % 2
    far_x, far_y = core % 2, 1 - core % 2

    def block_at(up, step_x, step_y):
        return ((z + up) % layers) * QUAD + ((y + step_y) % 2) * 2 + (x + step_x) % 2

    def device(block, which_core):
        return (block * seq_count + sequence, which_core)

    near = block_at(0, near_x, near_y)
    far = block_at(0, far_x, far_y)
    mate = SPAN - 1 - rank
    siblings = [(core + step) % tp_size for step in range(1, tp_size)]
    friends = [device(block_at(up, 0, 0), core) for up in range(1, layers)]
    friends += [device(near, core), device(far, core), device(mate, core)]
    friends += [device(rank, sibling) for sibling in siblings]

    barrier = pltpu.get_barrier_semaphore()
    for friend in friends:
        pl.semaphore_signal(barrier, inc=1, device_id=friend, device_id_type=MESH)
    pl.semaphore_wait(barrier, len(friends))

    def piece(block, owner):
        return blocks.at[block, pl.ds(pl.multiple_of(owner * part, part), part), :]

    def remote(source, target, send, recv, where):
        return pltpu.make_async_remote_copy(
            src_ref=source, dst_ref=target, send_sem=send, recv_sem=recv,
            device_id=where, device_id_type=MESH,
        )

    def ici(source, block, send, where):
        return remote(source, piece(block, core), send, ici_recv.at[block], where)

    def across(block, step):
        return remote(
            piece(block, core), piece(block, core), core_send.at[block, step - 1],
            core_recv.at[block, step - 1], device(rank, (core + step) % tp_size),
        )

    def arrival(block, step):
        giver = (core + tp_size - step) % tp_size
        return remote(
            piece(block, giver), piece(block, giver), core_send.at[block, step - 1],
            core_recv.at[block, step - 1], device(rank, giver),
        )

    def swap(source, target, index):
        return remote(source, target, swap_send.at[index], swap_recv.at[index], device(mate, core))

    give_heads = pl.ds((1 - side) * half_heads, half_heads)
    own_rows = pl.ds(pl.multiple_of(side * rows, rows), rows)
    mate_rows = pl.ds(pl.multiple_of((1 - side) * rows, rows), rows)
    swap(query_ref.at[give_heads], queries.at[:, own_rows, :], 0).start()
    own_piece = packed_ref.at[pl.ds(pl.multiple_of(core * part, part), part), :]
    for up in range(1, layers):
        ici(own_piece, rank, z_send.at[up - 1], device(block_at(up, 0, 0), core)).start()
    ici(own_piece, rank, near_send.at[0], device(near, core)).start()
    ici(own_piece, rank, far_send.at[0], device(far, core)).start()

    blocks[rank] = packed_ref[...]
    for head in range(half_heads):
        queries[head, own_rows, :] = query_ref[side * half_heads + head]
    peak_scr[...] = jnp.full(peak_scr.shape, masked_score, jnp.float32)
    total_scr[...] = jnp.zeros_like(total_scr)
    sum_scr[...] = jnp.zeros_like(sum_scr)

    def landed(block):
        ici(piece(block, core), block, near_send.at[0], device(near, core)).wait_recv()

    def hand_over(block):
        for step in range(1, tp_size):
            across(block, step).start()

    def pump(turn):
        group, up = turn // layers, turn % layers

        @pl.when(group == 0)
        def _():
            block = block_at(up, 0, 0)
            landed(block)
            ici(piece(block, core), block, near_send.at[up], device(near, core)).start()
            ici(piece(block, core), block, far_send.at[up], device(far, core)).start()
            hand_over(block)

        @pl.when(group == 1)
        def _():
            block = block_at(up, near_x, near_y)
            landed(block)
            ici(piece(block, core), block, far_send.at[layers + up], device(far, core)).start()
            hand_over(block)
            other = block_at(up, far_x, far_y)
            landed(other)
            hand_over(other)

        @pl.when(group == 3)
        def _():
            block = block_at(up, 1, 1)
            landed(block)
            hand_over(block)

    own_cols = pl.ds(pl.multiple_of(side * own_width, own_width), own_width)

    def unit(block, both, masked):
        held = slice(0, 2 * rows) if both else slice(rows, 2 * rows)
        count = 2 * rows if both else rows
        latent = blocks[block, :, :latent_width]
        rotary = blocks[block, :, latent_width:]
        keys = jnp.dot(
            latent, w_key_ref[:, own_cols], preferred_element_type=jnp.float32
        ).astype(jnp.bfloat16)
        values = jnp.dot(
            latent, w_value_ref[:, own_cols], preferred_element_type=jnp.float32
        ).astype(jnp.bfloat16)
        if masked:
            row = lax.broadcasted_iota(jnp.int32, (count, rows), 0)
            column = lax.broadcasted_iota(jnp.int32, (count, rows), 1)
            allowed = column <= row
        for head in range(half_heads):
            cols = slice(head * NOPE, (head + 1) * NOPE)
            scores = lax.dot_general(
                queries[head, held, :],
                jnp.concatenate([keys[:, cols], rotary], axis=1),
                (((1,), (1,)), ((), ())),
                preferred_element_type=jnp.float32,
            )
            if masked:
                scores = jnp.where(allowed, scores, masked_score)
            old = peak_scr[head, held, :1]
            peak = jnp.maximum(old, jnp.max(scores, axis=1, keepdims=True))
            expo = jnp.exp2((scores - peak) * factor)
            shrink = jnp.exp2((old - peak) * factor)
            total = total_scr[head, held, :1] * shrink + jnp.sum(expo, axis=1, keepdims=True)
            summed = jnp.dot(
                expo.astype(jnp.bfloat16), values[:, cols], preferred_element_type=jnp.float32
            )
            sum_scr[head, held, :] = sum_scr[head, held, :] * shrink + summed
            peak_scr[head, held, :] = jnp.broadcast_to(peak, (count, 128))
            total_scr[head, held, :] = jnp.broadcast_to(total, (count, 128))

    swap(query_ref.at[give_heads], queries.at[:, mate_rows, :], 0).wait_recv()

    def turn_body(turn, unused):
        group, up = turn // layers, turn % layers
        block = block_at(up, group % 2, group // 2)

        @pl.when(turn >= 1)
        def _():
            @pl.when(turn < SPAN - 1)
            def _():
                pump(turn + 1)

            for step in range(1, tp_size):
                arrival(block, step).wait_recv()

        @pl.when(block < low)
        def _():
            unit(block, True, False)

        @pl.when(block == low)
        def _():
            unit(block, True, True)

        @pl.when((block > low) & (block < high))
        def _():
            unit(block, False, False)

        @pl.when(block == high)
        def _():
            unit(block, False, True)

        @pl.when(turn == 0)
        def _():
            pump(turn + 1)

        return unused

    lax.fori_loop(0, SPAN, turn_body, 0)

    lane = lax.broadcasted_iota(jnp.int32, (rows, 128), 1)

    def finish(which):
        logs = jnp.zeros((rows, 128), jnp.float32)
        pieces = []
        for head in range(half_heads):
            total = total_scr[head, which, :]
            pieces.append((sum_scr[head, which, :] / total).astype(jnp.bfloat16))
            logs = jnp.where(lane == head, peak_scr[head, which, :] * scale + jnp.log(total), logs)
        return jnp.concatenate(pieces, axis=1), jnp.transpose(logs)[: log_give.shape[0]]

    give[...], log_give[...] = finish(mate_rows)
    swap(give, take, 1).start()
    swap(log_give, log_take, 2).start()
    attended, logs = finish(own_rows)
    out_ref[:, own_cols] = attended
    log_ref[side] = logs
    swap(give, take, 1).wait_recv()
    swap(log_give, log_take, 2).wait_recv()
    mate_cols = pl.ds(pl.multiple_of((1 - side) * own_width, own_width), own_width)
    out_ref[:, mate_cols] = take[...]
    log_ref[1 - side] = log_take[...]

    swap(query_ref.at[give_heads], queries.at[:, own_rows, :], 0).wait_send()
    swap(give, take, 1).wait_send()
    swap(log_give, log_take, 2).wait_send()
    for up in range(1, layers):
        ici(own_piece, rank, z_send.at[up - 1], device(near, core)).wait_send()
    for up in range(layers):
        ici(own_piece, rank, near_send.at[up], device(near, core)).wait_send()
    for up in range(2 * layers):
        ici(own_piece, rank, far_send.at[up], device(far, core)).wait_send()

    def drain(turn, unused):
        group, up = turn // layers, turn % layers
        block = block_at(up, group % 2, group // 2)
        for step in range(1, tp_size):
            across(block, step).wait_send()
        return unused

    lax.fori_loop(1, SPAN, drain, 0)


def attention(seq_count, tp_size, query, packed, w_key, w_value):
    heads, rows, depth = query.shape
    half = heads // 2
    padded = -(-half // 8) * 8
    vmem = pl.BlockSpec(memory_space=pltpu.VMEM)
    dma = pltpu.SemaphoreType.DMA
    return pl.pallas_call(
        functools.partial(attend_kernel, seq_count, tp_size),
        out_shape=(
            jax.ShapeDtypeStruct((rows, heads * VDIM), jnp.bfloat16),
            jax.ShapeDtypeStruct((2, padded, rows), jnp.float32),
        ),
        in_specs=[vmem] * 4,
        out_specs=(vmem, vmem),
        scratch_shapes=[
            pltpu.VMEM((SPAN,) + packed.shape, jnp.bfloat16),
            pltpu.VMEM((half, 2 * rows, depth), jnp.bfloat16),
            pltpu.VMEM((half, 2 * rows, 128), jnp.float32),
            pltpu.VMEM((half, 2 * rows, 128), jnp.float32),
            pltpu.VMEM((half, 2 * rows, VDIM), jnp.float32),
            pltpu.VMEM((rows, half * VDIM), jnp.bfloat16),
            pltpu.VMEM((rows, half * VDIM), jnp.bfloat16),
            pltpu.VMEM((padded, rows), jnp.float32),
            pltpu.VMEM((padded, rows), jnp.float32),
            dma((SPAN,)),
            dma((SPAN, tp_size - 1)),
            dma((SPAN // QUAD - 1,)),
            dma((SPAN // QUAD,)),
            dma((2 * SPAN // QUAD,)),
            dma((SPAN, tp_size - 1)),
            dma((3,)),
            dma((3,)),
        ],
        compiler_params=pltpu.CompilerParams(
            vmem_limit_bytes=56000 * 1024, collective_id=0, has_side_effects=True
        ),
        cost_estimate=pl.CostEstimate(
            flops=20 * 10**9, bytes_accessed=10**7, transcendentals=10**7
        ),
    )(query, packed, w_key, w_value)


def per_device(
    tokens,
    mix_gain,
    w_pool_in,
    w_qlat,
    w_kvlat,
    w_krope,
    q_gain,
    kv_gain,
    w_q_content,
    w_q_rotary,
    w_key,
    w_value,
    pool_mix,
    pool_scale,
    w_out_pool,
    w_out_attn,
):
    tp_size = lax.axis_size("tp")
    tp_rank = lax.axis_index("tp")
    sp_rank = lax.axis_index("sp")
    seq_count = lax.axis_size("sp") // SPAN
    local_rows, own_width = tokens.shape
    model_width = own_width * tp_size
    seq_rank = sp_rank // seq_count
    pool_cols = w_pool_in.shape[1]
    query_cols = w_qlat.shape[1]
    latent_cols = w_kvlat.shape[1]
    weight_cat = jnp.concatenate([w_pool_in, w_qlat, w_kvlat, w_krope], axis=1)
    raw_values = tokens.astype(jnp.float32)
    own_gain = lax.dynamic_slice_in_dim(mix_gain, tp_rank * own_width, own_width)
    squares = lax.psum(jnp.sum(raw_values * raw_values, axis=1), "tp")
    scaled = (raw_values * own_gain).astype(jnp.bfloat16)
    projected = jnp.dot(
        lax.all_gather(scaled, "tp", axis=1, tiled=True),
        weight_cat,
        preferred_element_type=jnp.float32,
    )
    inverse_rms = lax.rsqrt(squares / model_width + eps_norm)
    projected = (projected * inverse_rms[:, None]).astype(jnp.bfloat16)
    pool_pre = projected[:, :pool_cols]
    query_part = projected[:, pool_cols : pool_cols + query_cols]
    latent_part = projected[:, pool_cols + query_cols : pool_cols + query_cols + latent_cols]
    rotary_raw = projected[:, pool_cols + query_cols + latent_cols :]
    query_latent, kv_latent = (
        lax.all_gather(query_part, "tp", axis=1, tiled=True),
        lax.all_gather(latent_part, "tp", axis=1, tiled=True),
    )
    positions = seq_rank * local_rows + jnp.arange(local_rows, dtype=jnp.int32)
    query_normed = latent_norm(query_latent, q_gain)
    key_normed = latent_norm(kv_latent, kv_gain)
    own_heads = w_key.shape[1] // NOPE
    cosine, sine_table = tables(positions, ROPE)
    query_content = (
        jnp.dot(query_normed, w_q_content, preferred_element_type=jnp.float32)
        .astype(jnp.bfloat16)
        .reshape(local_rows, own_heads, NOPE)
    )
    query_rotary = rotate(
        jnp.dot(query_normed, w_q_rotary, preferred_element_type=jnp.float32).reshape(
            local_rows, own_heads, ROPE
        ),
        cosine[:, None, :],
        sine_table[:, None, :],
    ).astype(jnp.bfloat16)
    key_rotary = rotate(rotary_raw.astype(jnp.float32), cosine, sine_table).astype(jnp.bfloat16)
    query = jnp.concatenate(
        [
            query_content,
            query_rotary,
            jnp.zeros((local_rows, own_heads, 2 * NOPE - NOPE - ROPE), jnp.bfloat16),
        ],
        axis=-1,
    ).transpose(1, 0, 2)
    packed = jnp.concatenate(
        [key_normed, key_rotary, jnp.zeros((local_rows, NOPE - ROPE), jnp.bfloat16)], axis=1
    )
    attended, log_rows = attention(seq_count, tp_size, query, packed, w_key, w_value)
    log_total = log_rows[:, : own_heads // 2].reshape(own_heads, local_rows).T
    group_count = pool_cols // GROUP_DIM
    rim_rows = shifted(pool_pre[local_rows - (WIDEST - 1) :], "sp", seq_count)
    rim_rows = jnp.where(seq_rank > 0, rim_rows, jnp.zeros_like(rim_rows))
    pool_values = pool_pre.astype(jnp.float32)
    extended = jnp.concatenate([rim_rows.astype(jnp.float32), pool_values], axis=0)
    groups = tp_rank * group_count + jnp.arange(pool_cols, dtype=jnp.int32) // GROUP_DIM
    windows = jnp.left_shift(jnp.int32(2), groups % 4)
    window_sums = jnp.zeros((local_rows, pool_cols), jnp.float32)
    for distance in range(WIDEST):
        window_sums = window_sums + jnp.where(
            distance < windows[None, :],
            extended[WIDEST - 1 - distance : WIDEST - 1 - distance + local_rows],
            0.0,
        )
    counts = jnp.minimum(positions[:, None] + 1, windows[None, :]).astype(jnp.float32)
    pooled = (window_sums / counts - pool_values).astype(jnp.bfloat16)
    own_mix = lax.dynamic_slice_in_dim(pool_mix, tp_rank * group_count, group_count, 0)
    mixed_pool = jnp.einsum(
        "rgc,gcd->rgd",
        pooled.reshape(local_rows, group_count, GROUP_DIM),
        own_mix,
        preferred_element_type=jnp.float32,
    ).reshape(local_rows, pool_cols)
    own_scale = lax.dynamic_slice_in_dim(pool_scale, tp_rank * pool_cols, pool_cols)
    pool_out = (mixed_pool * own_scale).astype(jnp.bfloat16)
    layer_out = lax.psum_scatter(
        (
            jnp.dot(pool_out, w_out_pool, preferred_element_type=jnp.float32)
            + jnp.dot(attended, w_out_attn, preferred_element_type=jnp.float32)
        ).astype(jnp.bfloat16),
        "tp",
        scatter_dimension=0,
        tiled=True,
    )
    return (layer_out, log_total)


def solution(mesh):
    in_specs = (
        P("sp", "tp"),
        P(),
        P(None, "tp"),
        P(None, "tp"),
        P(None, "tp"),
        P(),
        P(),
        P(),
        P(None, "tp"),
        P(None, "tp"),
        P(None, "tp"),
        P(None, "tp"),
        P(),
        P(),
        P("tp", None),
        P("tp", None),
    )
    out_specs = (P(("sp", "tp"), None), P("sp", "tp"))
    return jax.shard_map(
        per_device, mesh=mesh, in_specs=in_specs, out_specs=out_specs, check_vma=False
    )
```

profile of v0, /device:TPU:0, one launch (start us, length us, event | category | flops | bytes accessed | tf_op | source)
XLA Modules:
  0.0 234.0 jit_solution(14276226565026381942)
XLA Ops:
  7.3 0.8 dynamic_slice.10
  8.1 2.2 fusion.15
  11.0 2.6 %psum.7 = f32[384]{0:T(512)S(1)} all-reduce(f32[384]{0:T(512)S(1)} %get-tuple-element.12), channel_id=1, replica_groups=mesh['sp'=16,'tp'=2] {'tp'}, use_global_device_ids=true, to_apply=%region_1.2 | all-reduce | flops 384 | bytes 3072 | tf_op jit(solution)/shard_map/psum | solution.py:377
  17.2 5.9 %all-gather.2.cloned.1.call-done = bf16[384,2048]{1,0:T(8,128)(2,1)} async-done(((bf16[384,1024]{1,0:T(8,128)(2,1)}), bf16[384,2048]{1,0:T(8,128)(2,1)}) %all-gather.2.cloned.1.call-update) | async-done | bytes 1572880 | tf_op jit(solution)/shard_map/all_gather | solution.py:380
  23.0 4.9 %fusion.11 = bf16[384,1088]{1,0:T(8,128)(2,1)S(1)} fusion(bf16[384,2048]{1,0:T(8,128)(2,1)} %all-gather.2.cloned.1.call-done, bf16[2048,64]{1,0:T(8,128)(2,1)S(1)} %copy.32, bf16[2048,256]{1,0:T(8,128)(2,1)} %param.20, bf16[2048,256]{1,0:T(8,128)(2,1)} %param.19, bf16[2048,512]{1,0:T(8,128)(2,1)} %param.18, f32[384]{0:T(512)S(1)} %add_rsqrt_fusion.2), kind=kOutput, calls=%fused_computation.24 | convolution fusion | flops 1729937408 | bytes 6866432 | tf_op jit(solution)/shard_map/dot_general | solution.py:379
  28.1 3.8 %collective-permute-start = (bf16[15,512]{1,0:T(8,128)(2,1)S(1)}, bf16[15,512]{1,0:T(8,128)(2,1)S(1)}, u32[]{:S(2)}, u32[]{:S(2)}) collective-permute-start(bf16[15,512]{1,0:T(8,128)(2,1)S(1)} %slice.102), channel_id=1, source_target_pairs={{0,2},{2,4},{4,6},{6,8},{8,10},{10,12},{12,14},{14,16},{16,18},{18... | collective-permute-start | bytes 46088 | tf_op jit(solution)/shard_map/ppermute | solution.py:28
  31.8 2.1 all_gather.11
  34.1 2.2 all_gather.10
  37.1 1.0 fusion.89
  38.1 1.5 convolution_convert_fusion
  39.6 1.5 copy.35
  41.1 1.2 copy.40
  42.2 2.7 %copy.45 = f32[384,8,32]{2,0,1:T(8,128)} copy(f32[384,8,32]{0,2,1:T(8,128)} %get-tuple-element.10) | data formatting | bytes 786432
  45.0 1.6 copy.44
  46.7 0.8 subtract_convert_fusion.1
  47.6 0.9 maximum_maximum_fusion.packed_ref
  48.5 1.9 subtract_convert_fusion
  50.4 1.8 maximum_bitcast_fusion.query_ref
  52.2 142.4 %shard_map.167 = (bf16[384,1024]{1,0:T(8,128)(2,1)}, f32[2,8,384]{2,1,0:T(8,128)}) custom-call(bf16[8,384,256]{2,1,0:T(8,128)(2,1)} %maximum_bitcast_fusion.query_ref, bf16[384,640]{1,0:T(8,128)(2,1)} %maximum_maximum_fusion.packed_ref, bf16[512,1024]{1,0:T(8,128)(2,1)} %w_key_ref.1, bf16[512,1024]{1,0:T(8,128)(2,1)} %w_value_ref.1), custom_call_target="tpu_custom_call" | custom-call | flops 20000000000 | bytes 10000000 | tf_op jit(solution)/shard_map/pallas_call | solution.py:310
  194.7 2.9 %fusion.90 = f32[384,2048]{1,0:T(8,128)S(1)} fusion(bf16[384,1024]{1,0:T(8,128)(2,1)} %get-tuple-element.4, bf16[1024,2048]{1,0:T(8,128)(2,1)S(1)} %copy-done.11), kind=kOutput, calls=%fused_computation.159 | convolution fusion | flops 1610612736 | bytes 8126464 | tf_op jit(solution)/shard_map/dot_general | solution.py:453
  197.6 1.1 slice_convert_fusion
  198.9 2.1 fusion.70
  201.2 2.2 add_convert_fusion
  204.0 23.1 %reduce-scatter.2.cloned.1.call-done = bf16[192,2048]{1,0:T(8,128)(2,1)} async-done(((bf16[384,2048]{1,0:T(8,128)(2,1)}), bf16[192,2048]{1,0:T(8,128)(2,1)}) %reduce-scatter.2.cloned.1.call-update) | async-done | bytes 786448 | tf_op jit(solution)/shard_map/reduce_scatter | solution.py:450
  (88 shorter events, 6.2 us)
Async XLA Ops:
  7.2 194.0 %copy-start = (bf16[512,2048]{1,0:T(8,128)(2,1)S(1)}, bf16[512,2048]{1,0:T(8,128)(2,1)}, u32[]{:S(2)}) copy-start(bf16[512,2048]{1,0:T(8,128)(2,1)} %param.30) | copy-start | bytes 6291460
  7.2 3.7 %copy-start.10 = (f32[1024]{0:T(1024)S(1)}, f32[1024]{0:T(1024)}, u32[]{:S(2)}) copy-start(f32[1024]{0:T(1024)} %param.29) | copy-start | bytes 12292
  7.2 15.8 %all-gather.2.cloned.1.call-start = ((), (), s32[]{:S(2)}) async-start(), calls=%async_computation.1 | async-start | bytes 2359296 | tf_op jit(solution)/shard_map/all_gather | solution.py:380
  10.4 216.8 %reduce-scatter.2.cloned.1.call-start = ((), (), s32[]{:S(2)}) async-start(), calls=%async_computation.2 | async-start | bytes 2359296 | tf_op jit(solution)/shard_map/reduce_scatter | solution.py:450
  27.9 9.1 %copy-start.4 = (bf16[384,1088]{1,0:T(8,128)(2,1)}, bf16[384,1088]{1,0:T(8,128)(2,1)S(1)}, u32[]{:S(2)}) copy-start(bf16[384,1088]{1,0:T(8,128)(2,1)S(1)} %fusion.11) | copy-start | bytes 2506756
  28.0 8.5 %copy-start.5 = (bf16[512,512]{1,0:T(8,128)(2,1)S(1)}, bf16[512,512]{1,0:T(8,128)(2,1)}, u32[]{:S(2)}) copy-start(bf16[512,512]{1,0:T(8,128)(2,1)} %param.25) | copy-start | bytes 1572868
  28.0 8.5 %copy-start.8 = (f32[512]{0:T(512)S(1)}, f32[512]{0:T(512)}, u32[]{:S(2)}) copy-start(f32[512]{0:T(512)} %param.22) | copy-start | bytes 6148
  28.1 170.7 %collective-permute-start = (bf16[15,512]{1,0:T(8,128)(2,1)S(1)}, bf16[15,512]{1,0:T(8,128)(2,1)S(1)}, u32[]{:S(2)}, u32[]{:S(2)}) collective-permute-start(bf16[15,512]{1,0:T(8,128)(2,1)S(1)} %slice.102), channel_id=1, source_target_pairs={{0,2},{2,4},{4,6},{6,8},{8,10},{10,12},{12,14},{14,16},{16,18},{18... | collective-permute-start | bytes 46088 | tf_op jit(solution)/shard_map/ppermute | solution.py:28
  34.1 4.0 %copy-start.12 = (bf16[512,1024]{1,0:T(8,128)(2,1)S(1)}, bf16[512,1024]{1,0:T(8,128)(2,1)}, u32[]{:S(2)}) copy-start(bf16[512,1024]{1,0:T(8,128)(2,1)} %param.24) | copy-start | bytes 3145732
  42.2 4.3 %copy-start.9 = (f32[512]{0:T(512)S(1)}, f32[512]{0:T(512)}, u32[]{:S(2)}) copy-start(f32[512]{0:T(512)} %param.23) | copy-start | bytes 6148
  52.2 142.4 %copy-start.11 = (bf16[1024,2048]{1,0:T(8,128)(2,1)S(1)}, bf16[1024,2048]{1,0:T(8,128)(2,1)}, u32[]{:S(2)}) copy-start(bf16[1024,2048]{1,0:T(8,128)(2,1)} %param.31) | copy-start | bytes 12582916
  194.6 4.2 %copy-start.13 = (bf16[8,128,128]{2,1,0:T(8,128)(2,1)S(1)}, bf16[8,128,128]{2,1,0:T(8,128)(2,1)}, u32[]{:S(2)}) copy-start(bf16[8,128,128]{2,1,0:T(8,128)(2,1)} %param.28) | copy-start | bytes 786436
  194.6 4.2 %copy-start.14 = (pred[512]{0:T(512)(128)(4,1)S(1)}, pred[512]{0:T(512)(128)(4,1)}, u32[]{:S(2)}) copy-start(pred[512]{0:T(512)(128)(4,1)} %get-tuple-element.30) | copy-start | bytes 1540
  194.6 4.2 %copy-start.15 = (pred[512]{0:T(512)(128)(4,1)S(1)}, pred[512]{0:T(512)(128)(4,1)}, u32[]{:S(2)}) copy-start(pred[512]{0:T(512)(128)(4,1)} %get-tuple-element.31) | copy-start | bytes 1540
  194.6 4.2 %copy-start.16 = (pred[512]{0:T(512)(128)(4,1)S(1)}, pred[512]{0:T(512)(128)(4,1)}, u32[]{:S(2)}) copy-start(pred[512]{0:T(512)(128)(4,1)} %get-tuple-element.22) | copy-start | bytes 1540
  194.6 4.2 %copy-start.17 = (pred[512]{0:T(512)(128)(4,1)S(1)}, pred[512]{0:T(512)(128)(4,1)}, u32[]{:S(2)}) copy-start(pred[512]{0:T(512)(128)(4,1)} %get-tuple-element.23) | copy-start | bytes 1540
  194.6 4.2 %copy-start.18 = (pred[512]{0:T(512)(128)(4,1)S(1)}, pred[512]{0:T(512)(128)(4,1)}, u32[]{:S(2)}) copy-start(pred[512]{0:T(512)(128)(4,1)} %get-tuple-element.32) | copy-start | bytes 1540
  194.6 4.2 %copy-start.19 = (pred[512]{0:T(512)(128)(4,1)S(1)}, pred[512]{0:T(512)(128)(4,1)}, u32[]{:S(2)}) copy-start(pred[512]{0:T(512)(128)(4,1)} %get-tuple-element.33) | copy-start | bytes 1540
  194.6 4.2 %copy-start.20 = (pred[512]{0:T(512)(128)(4,1)S(1)}, pred[512]{0:T(512)(128)(4,1)}, u32[]{:S(2)}) copy-start(pred[512]{0:T(512)(128)(4,1)} %get-tuple-element.20) | copy-start | bytes 1540
  194.7 4.2 %copy-start.21 = (pred[512]{0:T(512)(128)(4,1)S(1)}, pred[512]{0:T(512)(128)(4,1)}, u32[]{:S(2)}) copy-start(pred[512]{0:T(512)(128)(4,1)} %get-tuple-element.21) | copy-start | bytes 1540
  194.7 4.2 %copy-start.22 = (pred[512]{0:T(512)(128)(4,1)S(1)}, pred[512]{0:T(512)(128)(4,1)}, u32[]{:S(2)}) copy-start(pred[512]{0:T(512)(128)(4,1)} %get-tuple-element.26) | copy-start | bytes 1540
  194.7 4.2 %copy-start.23 = (pred[512]{0:T(512)(128)(4,1)S(1)}, pred[512]{0:T(512)(128)(4,1)}, u32[]{:S(2)}) copy-start(pred[512]{0:T(512)(128)(4,1)} %get-tuple-element.27) | copy-start | bytes 1540
  194.7 4.2 %copy-start.24 = (pred[512]{0:T(512)(128)(4,1)S(1)}, pred[512]{0:T(512)(128)(4,1)}, u32[]{:S(2)}) copy-start(pred[512]{0:T(512)(128)(4,1)} %get-tuple-element.18) | copy-start | bytes 1540
  194.7 4.2 %copy-start.25 = (pred[512]{0:T(512)(128)(4,1)S(1)}, pred[512]{0:T(512)(128)(4,1)}, u32[]{:S(2)}) copy-start(pred[512]{0:T(512)(128)(4,1)} %get-tuple-element.19) | copy-start | bytes 1540
  (5 other events, 12.2 us)
Sparse Core Ops, SparseCore 0:
  10.5 12.5 all-gather.1
  203.5 23.5 reduce-scatter.1
where the time goes:
time: 234 us
  Pallas kernels  142 us (61%)
  waiting for transfers between devices  29 us (12%)
  between operations  14.6 us (6%)
  matrix products  14.2 us (6%)
  other arithmetic  12.9 us (6%)
  local copies, waits for them, and re-layouts  10.1 us (4%)
  blocking collectives  6.91 us (3%)
  starting transfers between devices  3.85 us (2%)
    pallas_call x1, Pallas kernels, attention(): pl.pallas_call(functools.partial(attend_kernel, seq_count, tp_size), out_...  142 us
    reduce_scatter x1, waiting for transfers between devices, per_device(): lax.psum_scatter((jnp.dot(pool_out, w_out_pool, preferred_element_type=jn...  23.1 us
    all_gather x1, waiting for transfers between devices, per_device(): lax.all_gather(scaled, 'tp', axis=1, tiled=True)  5.88 us
    dot_general x1, matrix products, per_device(): jnp.dot(lax.all_gather(scaled, 'tp', axis=1, tiled=True), weight_cat, pre...  4.9 us
    unnamed x55, local copies, waits for them, and re-layouts  4.77 us
  transfers between devices with their start and end apart: 3, of which 2 were waited for; matrix products, arithmetic and copies ran while one was open for 11% of the time, Pallas kernels for 61%

commit v1 on v0

--- a/solution.py
+++ b/solution.py
@@ -132,12 +132,13 @@
     give_heads = pl.ds((1 - side) * half_heads, half_heads)
     own_rows = pl.ds(pl.multiple_of(side * rows, rows), rows)
     mate_rows = pl.ds(pl.multiple_of((1 - side) * rows, rows), rows)
-    swap(query_ref.at[give_heads], queries.at[:, own_rows, :], 0).start()
     own_piece = packed_ref.at[pl.ds(pl.multiple_of(core * part, part), part), :]
     for up in range(1, layers):
         ici(own_piece, rank, z_send.at[up - 1], device(block_at(up, 0, 0), core)).start()
     ici(own_piece, rank, near_send.at[0], device(near, core)).start()
     ici(own_piece, rank, far_send.at[0], device(far, core)).start()
+
+    swap(query_ref.at[give_heads], queries.at[:, own_rows, :], 0).start()
 
     blocks[rank] = packed_ref[...]
     for head in range(half_heads):
@@ -219,18 +220,20 @@
             peak_scr[head, held, :] = jnp.broadcast_to(peak, (count, 128))
             total_scr[head, held, :] = jnp.broadcast_to(total, (count, 128))
 
+    for up in range(1, layers):
+        pump(up)
     swap(query_ref.at[give_heads], queries.at[:, mate_rows, :], 0).wait_recv()
 
     def turn_body(turn, unused):
         group, up = turn // layers, turn % layers
         block = block_at(up, group % 2, group // 2)
 
+        @pl.when(turn < SPAN - layers)
+        def _():
+            pump(turn + layers)
+
         @pl.when(turn >= 1)
         def _():
-            @pl.when(turn < SPAN - 1)
-            def _():
-                pump(turn + 1)
-
             for step in range(1, tp_size):
                 arrival(block, step).wait_recv()
 
@@ -249,10 +252,6 @@
         @pl.when(block == high)
         def _():
             unit(block, False, True)
-
-        @pl.when(turn == 0)
-        def _():
-            pump(turn + 1)
 
         return unused
 

time: 234 us -> 237 us (1.013)
  waiting for transfers between devices: 29 us -> 44.4 us
  Pallas kernels: 142 us -> 130 us
    reduce_scatter x1, waiting for transfers between devices: 23.1 us -> 38.5 us  [per_device(): lax.psum_scatter((jnp.dot(pool_out, w_out_pool, preferred_element_type=jn...]
    pallas_call x1, Pallas kernels: 142 us -> 130 us  [attention(): pl.pallas_call(functools.partial(attend_kernel, seq_count, tp_size), out_...]
  transfers between devices with their start and end apart: 3 -> 3, of which waited for: 2 -> 2; matrix products, arithmetic and copies ran while one was open for 11% -> 10% of each run, Pallas kernels for 61% -> 55%
where the time goes in v1:
time: 237 us
  Pallas kernels  130 us (55%)
  waiting for transfers between devices  44.4 us (19%)
  between operations  14.6 us (6%)
  matrix products  14.2 us (6%)
  other arithmetic  12.9 us (5%)
  local copies, waits for them, and re-layouts  10.1 us (4%)
  blocking collectives  6.91 us (3%)
  starting transfers between devices  3.85 us (2%)
    pallas_call x1, Pallas kernels, attention(): pl.pallas_call(functools.partial(attend_kernel, seq_count, tp_size), out_...  130 us
    reduce_scatter x1, waiting for transfers between devices, per_device(): lax.psum_scatter((jnp.dot(pool_out, w_out_pool, preferred_element_type=jn...  38.5 us
    all_gather x1, waiting for transfers between devices, per_device(): lax.all_gather(scaled, 'tp', axis=1, tiled=True)  5.88 us
    dot_general x1, matrix products, per_device(): jnp.dot(lax.all_gather(scaled, 'tp', axis=1, tiled=True), weight_cat, pre...  4.9 us
    unnamed x55, local copies, waits for them, and re-layouts  4.77 us
  transfers between devices with their start and end apart: 3, of which 2 were waited for; matrix products, arithmetic and copies ran while one was open for 10% of the time, Pallas kernels for 55%

profile of v1, /device:TPU:0, one launch (start us, length us, event | category | flops | bytes accessed | tf_op | source)
XLA Modules:
  0.0 237.0 jit_solution(8621504568686015043)
XLA Ops:
  7.3 0.8 dynamic_slice.10
  8.1 2.2 fusion.15
  11.0 2.6 %psum.7 = f32[384]{0:T(512)S(1)} all-reduce(f32[384]{0:T(512)S(1)} %get-tuple-element.12), channel_id=1, replica_groups=mesh['sp'=16,'tp'=2] {'tp'}, use_global_device_ids=true, to_apply=%region_1.2 | all-reduce | flops 384 | bytes 3072 | tf_op jit(solution)/shard_map/psum | solution.py:376
  17.2 5.9 %all-gather.2.cloned.1.call-done = bf16[384,2048]{1,0:T(8,128)(2,1)} async-done(((bf16[384,1024]{1,0:T(8,128)(2,1)}), bf16[384,2048]{1,0:T(8,128)(2,1)}) %all-gather.2.cloned.1.call-update) | async-done | bytes 1572880 | tf_op jit(solution)/shard_map/all_gather | solution.py:379
  23.0 4.9 %fusion.11 = bf16[384,1088]{1,0:T(8,128)(2,1)S(1)} fusion(bf16[384,2048]{1,0:T(8,128)(2,1)} %all-gather.2.cloned.1.call-done, bf16[2048,64]{1,0:T(8,128)(2,1)S(1)} %copy.32, bf16[2048,256]{1,0:T(8,128)(2,1)} %param.20, bf16[2048,256]{1,0:T(8,128)(2,1)} %param.19, bf16[2048,512]{1,0:T(8,128)(2,1)} %param.18, f32[384]{0:T(512)S(1)} %add_rsqrt_fusion.2), kind=kOutput, calls=%fused_computation.24 | convolution fusion | flops 1729937408 | bytes 6866432 | tf_op jit(solution)/shard_map/dot_general | solution.py:378
  28.1 3.8 %collective-permute-start = (bf16[15,512]{1,0:T(8,128)(2,1)S(1)}, bf16[15,512]{1,0:T(8,128)(2,1)S(1)}, u32[]{:S(2)}, u32[]{:S(2)}) collective-permute-start(bf16[15,512]{1,0:T(8,128)(2,1)S(1)} %slice.102), channel_id=1, source_target_pairs={{0,2},{2,4},{4,6},{6,8},{8,10},{10,12},{12,14},{14,16},{16,18},{18... | collective-permute-start | bytes 46088 | tf_op jit(solution)/shard_map/ppermute | solution.py:28
  31.8 2.1 all_gather.11
  34.1 2.2 all_gather.10
  37.1 1.0 fusion.89
  38.1 1.5 convolution_convert_fusion
  39.6 1.5 copy.35
  41.1 1.2 copy.40
  42.2 2.7 %copy.45 = f32[384,8,32]{2,0,1:T(8,128)} copy(f32[384,8,32]{0,2,1:T(8,128)} %get-tuple-element.10) | data formatting | bytes 786432
  45.0 1.6 copy.44
  46.7 0.8 subtract_convert_fusion.1
  47.6 0.9 maximum_maximum_fusion.packed_ref
  48.5 1.9 subtract_convert_fusion
  50.4 1.8 maximum_bitcast_fusion.query_ref
  52.2 130.0 %shard_map.167 = (bf16[384,1024]{1,0:T(8,128)(2,1)}, f32[2,8,384]{2,1,0:T(8,128)}) custom-call(bf16[8,384,256]{2,1,0:T(8,128)(2,1)} %maximum_bitcast_fusion.query_ref, bf16[384,640]{1,0:T(8,128)(2,1)} %maximum_maximum_fusion.packed_ref, bf16[512,1024]{1,0:T(8,128)(2,1)} %w_key_ref.1, bf16[512,1024]{1,0:T(8,128)(2,1)} %w_value_ref.1), custom_call_target="tpu_custom_call" | custom-call | flops 20000000000 | bytes 10000000 | tf_op jit(solution)/shard_map/pallas_call | solution.py:309
  182.3 2.9 %fusion.90 = f32[384,2048]{1,0:T(8,128)S(1)} fusion(bf16[384,1024]{1,0:T(8,128)(2,1)} %get-tuple-element.4, bf16[1024,2048]{1,0:T(8,128)(2,1)S(1)} %copy-done.11), kind=kOutput, calls=%fused_computation.159 | convolution fusion | flops 1610612736 | bytes 8126464 | tf_op jit(solution)/shard_map/dot_general | solution.py:452
  185.3 1.1 slice_convert_fusion
  186.5 2.1 fusion.70
  188.8 2.2 add_convert_fusion
  191.6 38.5 %reduce-scatter.2.cloned.1.call-done = bf16[192,2048]{1,0:T(8,128)(2,1)} async-done(((bf16[384,2048]{1,0:T(8,128)(2,1)}), bf16[192,2048]{1,0:T(8,128)(2,1)}) %reduce-scatter.2.cloned.1.call-update) | async-done | bytes 786448 | tf_op jit(solution)/shard_map/reduce_scatter | solution.py:449
  (88 shorter events, 6.2 us)
Async XLA Ops:
  7.2 181.6 %copy-start = (bf16[512,2048]{1,0:T(8,128)(2,1)S(1)}, bf16[512,2048]{1,0:T(8,128)(2,1)}, u32[]{:S(2)}) copy-start(bf16[512,2048]{1,0:T(8,128)(2,1)} %param.30) | copy-start | bytes 6291460
  7.2 3.7 %copy-start.10 = (f32[1024]{0:T(1024)S(1)}, f32[1024]{0:T(1024)}, u32[]{:S(2)}) copy-start(f32[1024]{0:T(1024)} %param.29) | copy-start | bytes 12292
  7.2 15.8 %all-gather.2.cloned.1.call-start = ((), (), s32[]{:S(2)}) async-start(), calls=%async_computation.1 | async-start | bytes 2359296 | tf_op jit(solution)/shard_map/all_gather | solution.py:379
  10.4 219.8 %reduce-scatter.2.cloned.1.call-start = ((), (), s32[]{:S(2)}) async-start(), calls=%async_computation.2 | async-start | bytes 2359296 | tf_op jit(solution)/shard_map/reduce_scatter | solution.py:449
  27.9 9.1 %copy-start.4 = (bf16[384,1088]{1,0:T(8,128)(2,1)}, bf16[384,1088]{1,0:T(8,128)(2,1)S(1)}, u32[]{:S(2)}) copy-start(bf16[384,1088]{1,0:T(8,128)(2,1)S(1)} %fusion.11) | copy-start | bytes 2506756
  28.0 8.5 %copy-start.5 = (bf16[512,512]{1,0:T(8,128)(2,1)S(1)}, bf16[512,512]{1,0:T(8,128)(2,1)}, u32[]{:S(2)}) copy-start(bf16[512,512]{1,0:T(8,128)(2,1)} %param.25) | copy-start | bytes 1572868
  28.0 8.5 %copy-start.8 = (f32[512]{0:T(512)S(1)}, f32[512]{0:T(512)}, u32[]{:S(2)}) copy-start(f32[512]{0:T(512)} %param.22) | copy-start | bytes 6148
  28.1 158.3 %collective-permute-start = (bf16[15,512]{1,0:T(8,128)(2,1)S(1)}, bf16[15,512]{1,0:T(8,128)(2,1)S(1)}, u32[]{:S(2)}, u32[]{:S(2)}) collective-permute-start(bf16[15,512]{1,0:T(8,128)(2,1)S(1)} %slice.102), channel_id=1, source_target_pairs={{0,2},{2,4},{4,6},{6,8},{8,10},{10,12},{12,14},{14,16},{16,18},{18... | collective-permute-start | bytes 46088 | tf_op jit(solution)/shard_map/ppermute | solution.py:28
  34.1 4.0 %copy-start.12 = (bf16[512,1024]{1,0:T(8,128)(2,1)S(1)}, bf16[512,1024]{1,0:T(8,128)(2,1)}, u32[]{:S(2)}) copy-start(bf16[512,1024]{1,0:T(8,128)(2,1)} %param.24) | copy-start | bytes 3145732
  42.2 4.3 %copy-start.9 = (f32[512]{0:T(512)S(1)}, f32[512]{0:T(512)}, u32[]{:S(2)}) copy-start(f32[512]{0:T(512)} %param.23) | copy-start | bytes 6148
  52.2 130.0 %copy-start.11 = (bf16[1024,2048]{1,0:T(8,128)(2,1)S(1)}, bf16[1024,2048]{1,0:T(8,128)(2,1)}, u32[]{:S(2)}) copy-start(bf16[1024,2048]{1,0:T(8,128)(2,1)} %param.31) | copy-start | bytes 12582916
  182.2 4.2 %copy-start.13 = (bf16[8,128,128]{2,1,0:T(8,128)(2,1)S(1)}, bf16[8,128,128]{2,1,0:T(8,128)(2,1)}, u32[]{:S(2)}) copy-start(bf16[8,128,128]{2,1,0:T(8,128)(2,1)} %param.28) | copy-start | bytes 786436
  182.2 4.2 %copy-start.14 = (pred[512]{0:T(512)(128)(4,1)S(1)}, pred[512]{0:T(512)(128)(4,1)}, u32[]{:S(2)}) copy-start(pred[512]{0:T(512)(128)(4,1)} %get-tuple-element.30) | copy-start | bytes 1540
  182.2 4.2 %copy-start.15 = (pred[512]{0:T(512)(128)(4,1)S(1)}, pred[512]{0:T(512)(128)(4,1)}, u32[]{:S(2)}) copy-start(pred[512]{0:T(512)(128)(4,1)} %get-tuple-element.31) | copy-start | bytes 1540
  182.2 4.2 %copy-start.16 = (pred[512]{0:T(512)(128)(4,1)S(1)}, pred[512]{0:T(512)(128)(4,1)}, u32[]{:S(2)}) copy-start(pred[512]{0:T(512)(128)(4,1)} %get-tuple-element.22) | copy-start | bytes 1540
  182.2 4.2 %copy-start.17 = (pred[512]{0:T(512)(128)(4,1)S(1)}, pred[512]{0:T(512)(128)(4,1)}, u32[]{:S(2)}) copy-start(pred[512]{0:T(512)(128)(4,1)} %get-tuple-element.23) | copy-start | bytes 1540
  182.2 4.2 %copy-start.18 = (pred[512]{0:T(512)(128)(4,1)S(1)}, pred[512]{0:T(512)(128)(4,1)}, u32[]{:S(2)}) copy-start(pred[512]{0:T(512)(128)(4,1)} %get-tuple-element.32) | copy-start | bytes 1540
  182.2 4.2 %copy-start.19 = (pred[512]{0:T(512)(128)(4,1)S(1)}, pred[512]{0:T(512)(128)(4,1)}, u32[]{:S(2)}) copy-start(pred[512]{0:T(512)(128)(4,1)} %get-tuple-element.33) | copy-start | bytes 1540
  182.3 4.2 %copy-start.20 = (pred[512]{0:T(512)(128)(4,1)S(1)}, pred[512]{0:T(512)(128)(4,1)}, u32[]{:S(2)}) copy-start(pred[512]{0:T(512)(128)(4,1)} %get-tuple-element.20) | copy-start | bytes 1540
  182.3 4.2 %copy-start.21 = (pred[512]{0:T(512)(128)(4,1)S(1)}, pred[512]{0:T(512)(128)(4,1)}, u32[]{:S(2)}) copy-start(pred[512]{0:T(512)(128)(4,1)} %get-tuple-element.21) | copy-start | bytes 1540
  182.3 4.2 %copy-start.22 = (pred[512]{0:T(512)(128)(4,1)S(1)}, pred[512]{0:T(512)(128)(4,1)}, u32[]{:S(2)}) copy-start(pred[512]{0:T(512)(128)(4,1)} %get-tuple-element.26) | copy-start | bytes 1540
  182.3 4.2 %copy-start.23 = (pred[512]{0:T(512)(128)(4,1)S(1)}, pred[512]{0:T(512)(128)(4,1)}, u32[]{:S(2)}) copy-start(pred[512]{0:T(512)(128)(4,1)} %get-tuple-element.27) | copy-start | bytes 1540
  182.3 4.2 %copy-start.24 = (pred[512]{0:T(512)(128)(4,1)S(1)}, pred[512]{0:T(512)(128)(4,1)}, u32[]{:S(2)}) copy-start(pred[512]{0:T(512)(128)(4,1)} %get-tuple-element.18) | copy-start | bytes 1540
  182.3 4.2 %copy-start.25 = (pred[512]{0:T(512)(128)(4,1)S(1)}, pred[512]{0:T(512)(128)(4,1)}, u32[]{:S(2)}) copy-start(pred[512]{0:T(512)(128)(4,1)} %get-tuple-element.19) | copy-start | bytes 1540
  (5 other events, 12.2 us)
Sparse Core Ops, SparseCore 0:
  10.5 12.5 all-gather.1
  191.1 38.9 reduce-scatter.1
